TPU v7x, 32 devices: a whole 2x2x4 slice. The times are simulated.
32 devices in a mesh: fs: 16 (over z, y, x), tp: 2 (over core).
Axes of the slice: x: 2, y: 2, z: 4, core: 2. Of those that a mesh axis runs over, the one named last changes fastest.
Arguments:
- tokens: bfloat16 [8192, 2048], P('fs', 'tp'), may hold values from -24 to 24
- u_weight: bfloat16 [2048, 1024], P('fs', 'tp'), may hold values from -0.125 to 0.125
- v_weight: bfloat16 [2048, 1024], P('fs', 'tp'), may hold values from -0.125 to 0.125
- sg_gain: float32 [1024], P('tp'), may hold values from 0.1 to 1.9
- spatial_weight: bfloat16 [8, 128, 128], P('tp'), may hold values from -0.5 to 0.5
- spatial_bias: float32 [8, 128], P('tp'), may hold values from 0.1 to 1.9
- out_weight: bfloat16 [1024, 2048], P('tp', 'fs'), may hold values from -0.1875 to 0.1875
- gain_one: float32 [2048], P('tp'), may hold values from 0.1 to 1.9
- gate_weight: bfloat16 [2048, 5632], P('fs', 'tp'), may hold values from -0.125 to 0.125
- up_weight: bfloat16 [2048, 5632], P('fs', 'tp'), may hold values from -0.125 to 0.125
- down_weight: bfloat16 [5632, 2048], P('tp', 'fs'), may hold values from -0.078125 to 0.078125
- gain_two: float32 [2048], P('tp'), may hold values from 0.1 to 1.9
Outputs:
- layer_out: bfloat16 [8192, 2048], P('fs', 'tp')
All inputs are finite; a program needn't handle non-finite values.
Results may differ from a plain program's by a relative error of at most 0.014.
Values may be sent and summed in bfloat16 or wider, within the bound.
A program may use at most 128 MiB of HBM per device.

v0:
```python
import jax
import jax.numpy as jnp
from jax import lax
from jax.sharding import PartitionSpec as P

EPS = 1e-05
ALPHA = 2.0**0.25


def add_rows(left, piece):
    return jnp.dot(left, piece, preferred_element_type=jnp.float32)


def scaled_rows(vals, sums, gain, count):
    mean = sums[0][:, None] / count
    square = sums[1][:, None] / count
    return (vals - mean) * lax.rsqrt(square - mean * mean + EPS) * gain[None, :]


def on_device(
    tokens,
    u_weight,
    v_weight,
    sg_gain,
    spatial_weight,
    spatial_bias,
    out_weight,
    gain_one,
    gate_weight,
    up_weight,
    down_weight,
    gain_two,
):
    parts = lax.axis_size("tp")
    whole = lax.all_gather(tokens, "tp", axis=1, tiled=True)
    rows = whole.shape[0]
    width_sg = u_weight.shape[1]

    def add_one(piece):
        return add_rows(whole, piece)

    pre_u = add_one(lax.all_gather(u_weight, "fs", axis=0, tiled=True))
    pre_v = add_one(lax.all_gather(v_weight, "fs", axis=0, tiled=True))
    gated = jax.nn.gelu(pre_u)
    valued = jax.nn.gelu(pre_v)
    stats = lax.psum((jnp.sum(valued, axis=1), jnp.sum(valued * valued, axis=1)), "tp")
    normed = scaled_rows(valued, stats, sg_gain, width_sg * parts).astype(jnp.bfloat16)
    groups_here = spatial_weight.shape[0]
    block = spatial_weight.shape[1]
    group_width = width_sg // groups_here
    shaped = normed.reshape(rows // block, block, groups_here, group_width)
    lower = jnp.tril(jnp.ones((block, block), jnp.bool_))
    masked = jnp.where(lower[None], spatial_weight, jnp.zeros_like(spatial_weight))
    mixed = jnp.einsum("gij,njgd->nigd", masked, shaped, preferred_element_type=jnp.float32)
    mixed = mixed + spatial_bias.T[None, :, :, None]
    gated_out = (gated * mixed.reshape(rows, width_sg)).astype(jnp.bfloat16)
    terms = jnp.dot(
        gated_out,
        lax.all_gather(out_weight, "fs", axis=1, tiled=True),
        preferred_element_type=jnp.float32,
    )
    mix = lax.psum_scatter(terms.astype(jnp.bfloat16), "tp", scatter_dimension=1, tiled=True)
    resid = ALPHA * tokens.astype(jnp.float32) + mix.astype(jnp.float32)
    first_sums = lax.psum((jnp.sum(resid, axis=1), jnp.sum(resid * resid, axis=1)), "tp")
    first = scaled_rows(resid, first_sums, gain_one, resid.shape[1] * parts).astype(jnp.bfloat16)
    whole_first = lax.all_gather(first, "tp", axis=1, tiled=True)

    def add_first(piece):
        return add_rows(whole_first, piece)

    gate = add_first(lax.all_gather(gate_weight, "fs", axis=0, tiled=True))
    upper = add_first(lax.all_gather(up_weight, "fs", axis=0, tiled=True))
    hidden = (jax.nn.silu(gate) * upper).astype(jnp.bfloat16)
    ffn_terms = jnp.dot(
        hidden,
        lax.all_gather(down_weight, "fs", axis=1, tiled=True),
        preferred_element_type=jnp.float32,
    )
    ffn = lax.psum_scatter(ffn_terms.astype(jnp.bfloat16), "tp", scatter_dimension=1, tiled=True)
    second = ALPHA * first.astype(jnp.float32) + ffn.astype(jnp.float32)
    last_sums = lax.psum((jnp.sum(second, axis=1), jnp.sum(second * second, axis=1)), "tp")
    return scaled_rows(second, last_sums, gain_two, second.shape[1] * parts).astype(jnp.bfloat16)


def solution(mesh):
    return jax.shard_map(
        on_device,
        mesh=mesh,
        in_specs=(
            P("fs", "tp"),
            P("fs", "tp"),
            P("fs", "tp"),
            P("tp"),
            P("tp", None, None),
            P("tp", None),
            P("tp", "fs"),
            P("tp"),
            P("fs", "tp"),
            P("fs", "tp"),
            P("tp", "fs"),
            P("tp"),
        ),
        out_specs=P("fs", "tp"),
        check_vma=False,
    )
```

profile of v0, /device:TPU:0, one launch (start us, length us, event | category | flops | bytes accessed | tf_op | source)
XLA Modules:
  0.0 759.9 jit_solution(2212430606449240204)
XLA Ops:
  6.5 0.0 all-gather.9.cloned.1.call-start
  6.5 0.7 all-gather.9.cloned.1.call-update
  7.3 0.0 all-gather.13.cloned.1.call-start
  7.3 0.7 all-gather.13.cloned.1.call-update
  8.0 0.0 all-gather.11.cloned.1.call-start
  8.1 0.7 all-gather.11.cloned.1.call-update
  8.7 0.0 all-gather.15.cloned.1.call-start
  8.8 0.5 all-gather.15.cloned.1.call-update
  9.3 0.0 reduce-scatter.3.cloned.1.call-start
  9.4 0.0 copy-start.7
  9.4 12.8 %all-gather.9.cloned.1.call-done = bf16[512,2048]{1,0:T(8,128)(2,1)} async-done(((bf16[512,1024]{1,0:T(8,128)(2,1)}), bf16[512,2048]{1,0:T(8,128)(2,1)}) %all-gather.9.cloned.1.call-update) | async-done | bytes 2097168 | tf_op jit(solution)/shard_map/all_gather | solution.py:35
  22.2 64.4 %all-gather.13.cloned.1.call-done = bf16[2048,512]{1,0:T(8,128)(2,1)} async-done(((bf16[128,512]{1,0:T(8,128)(2,1)}), bf16[2048,512]{1,0:T(8,128)(2,1)}) %all-gather.13.cloned.1.call-update) | async-done | bytes 2097168 | tf_op jit(solution)/shard_map/all_gather | solution.py:43
  86.6 3.8 fusion.35
  90.4 0.0 copy-start.8
  90.4 2.6 all-reduce.2
  93.0 0.4 multiply_convert_fusion.3
  93.5 0.1 reshape.41
  93.6 0.4 fusion.2
  94.0 0.4 copy.19
  94.4 54.1 %all-gather.11.cloned.1.call-done = bf16[2048,512]{1,0:T(8,128)(2,1)} async-done(((bf16[128,512]{1,0:T(8,128)(2,1)}), bf16[2048,512]{1,0:T(8,128)(2,1)}) %all-gather.11.cloned.1.call-update) | async-done | bytes 2097168 | tf_op jit(solution)/shard_map/all_gather | solution.py:42
  148.5 64.3 %all-gather.15.cloned.1.call-done = bf16[512,2048]{1,0:T(8,128)(2,1)} async-done(((bf16[512,128]{1,0:T(8,128)(2,1)}), bf16[512,2048]{1,0:T(8,128)(2,1)}) %all-gather.15.cloned.1.call-update) | async-done | bytes 2097168 | tf_op jit(solution)/shard_map/all_gather | solution.py:59
  212.9 6.8 convolution_convert_fusion.1
  219.7 0.0 reduce-scatter.3.cloned.1.call-update
  219.7 0.0 all-gather.17.cloned.1.call-start
  219.7 7.9 %reduce-scatter.3.cloned.1.call-done = bf16[512,1024]{1,0:T(8,128)(2,1)} async-done(((bf16[512,2048]{1,0:T(8,128)(2,1)}), bf16[512,1024]{1,0:T(8,128)(2,1)}) %reduce-scatter.3.cloned.1.call-update) | async-done | bytes 1048592 | tf_op jit(solution)/shard_map/reduce_scatter | solution.py:62
  227.6 1.9 fusion
  229.5 2.5 all-reduce.1
  232.0 1.5 multiply_convert_fusion.2
  233.6 0.0 all-gather.17.cloned.1.call-update
  233.6 0.0 all-gather.19.cloned.1.call-start
  233.6 0.7 all-gather.19.cloned.1.call-update
  234.3 0.0 all-gather.21.cloned.1.call-start
  234.4 0.7 all-gather.21.cloned.1.call-update
  235.1 0.0 all-gather.23.cloned.1.call-start
  235.1 0.7 all-gather.23.cloned.1.call-update
  235.8 0.2 reduce-scatter.5.cloned.1.call-start
  236.1 9.5 %all-gather.17.cloned.1.call-done = bf16[512,2048]{1,0:T(8,128)(2,1)} async-done(((bf16[512,1024]{1,0:T(8,128)(2,1)}), bf16[512,2048]{1,0:T(8,128)(2,1)}) %all-gather.17.cloned.1.call-update) | async-done | bytes 2097168 | tf_op jit(solution)/shard_map/all_gather | solution.py:66
  245.6 145.4 %all-gather.19.cloned.1.call-done = bf16[2048,2816]{1,0:T(8,128)(2,1)} async-done(((bf16[128,2816]{1,0:T(8,128)(2,1)}), bf16[2048,2816]{1,0:T(8,128)(2,1)}) %all-gather.19.cloned.1.call-update) | async-done | bytes 11534352 | tf_op jit(solution)/shard_map/all_gather | solution.py:71
  391.0 12.5 %fusion.38 = f32[512,2816]{1,0:T(8,128)} fusion(bf16[512,2048]{1,0:T(8,128)(2,1)} %all-gather.17.cloned.1.call-done, bf16[2048,2816]{1,0:T(8,128)(2,1)} %all-gather.19.cloned.1.call-done), kind=kOutput, calls=%fused_computation.57 | convolution fusion | flops 5905580032 | bytes 19398656 | tf_op jit(solution)/shard_map/dot_general | solution.py:11
  403.5 129.9 %all-gather.21.cloned.1.call-done = bf16[2048,2816]{1,0:T(8,128)(2,1)} async-done(((bf16[128,2816]{1,0:T(8,128)(2,1)}), bf16[2048,2816]{1,0:T(8,128)(2,1)}) %all-gather.21.cloned.1.call-update) | async-done | bytes 11534352 | tf_op jit(solution)/shard_map/all_gather | solution.py:72
  533.4 183.0 %all-gather.23.cloned.1.call-done = bf16[2816,2048]{1,0:T(8,128)(2,1)} async-done(((bf16[2816,128]{1,0:T(8,128)(2,1)}), bf16[2816,2048]{1,0:T(8,128)(2,1)}) %all-gather.23.cloned.1.call-update) | async-done | bytes 11534352 | tf_op jit(solution)/shard_map/all_gather | solution.py:76
  716.4 0.0 copy-done.9
  716.4 22.8 %convolution_convert_fusion = bf16[512,2048]{1,0:T(8,128)(2,1)} fusion(bf16[2816,2048]{1,0:T(8,128)(2,1)} %all-gather.23.cloned.1.call-done, f32[512,2816]{1,0:T(8,128)} %fusion.38, bf16[512,2048]{1,0:T(8,128)(2,1)S(1)} %copy-done.9, bf16[2048,2816]{1,0:T(8,128)(2,1)} %all-gather.21.cloned.1.call-done), kind=kOutput, calls=%fused_computation.1 | convolution fusion | flops 11820859392 | bytes 33030144 | tf_op jit(solution)/shard_map/dot_general | solution.py:74
  739.1 0.0 reduce-scatter.5.cloned.1.call-update
  739.2 8.0 %reduce-scatter.5.cloned.1.call-done = bf16[512,1024]{1,0:T(8,128)(2,1)} async-done(((bf16[512,2048]{1,0:T(8,128)(2,1)}), bf16[512,1024]{1,0:T(8,128)(2,1)}) %reduce-scatter.5.cloned.1.call-update) | async-done | bytes 1048592 | tf_op jit(solution)/shard_map/reduce_scatter | solution.py:79
  747.1 1.9 fusion.1
  749.0 2.5 all-reduce
  751.5 1.5 multiply_convert_fusion.1
  (21 shorter events, 0.1 us)
Async XLA Ops:
  6.5 15.7 %all-gather.9.cloned.1.call-start = ((), (), s32[]{:S(2)}) async-start(), calls=%async_computation.2 | async-start | bytes 3145728 | tf_op jit(solution)/shard_map/all_gather | solution.py:35
  7.3 79.3 %all-gather.13.cloned.1.call-start = ((), (), s32[]{:S(2)}) async-start(), calls=%async_computation.4 | async-start | bytes 2228224 | tf_op jit(solution)/shard_map/all_gather | solution.py:43
  8.0 140.5 %all-gather.11.cloned.1.call-start = ((), (), s32[]{:S(2)}) async-start(), calls=%async_computation.3 | async-start | bytes 2228224 | tf_op jit(solution)/shard_map/all_gather | solution.py:42
  8.7 204.1 %all-gather.15.cloned.1.call-start = ((), (), s32[]{:S(2)}) async-start(), calls=%async_computation.5 | async-start | bytes 2228224 | tf_op jit(solution)/shard_map/all_gather | solution.py:59
  9.3 218.3 %reduce-scatter.3.cloned.1.call-start = ((), (), s32[]{:S(2)}) async-start(), calls=%async_computation.6 | async-start | bytes 3145728 | tf_op jit(solution)/shard_map/reduce_scatter | solution.py:62
  9.4 83.7 %copy-start.7 = (f32[512]{0:T(512)S(1)}, f32[512]{0:T(512)}, u32[]{:S(2)}) copy-start(f32[512]{0:T(512)} %param.15) | copy-start | bytes 6148
  90.4 3.2 copy-start.4
  90.4 3.2 copy-start.8
  219.7 8.0 %copy-start.1 = (bf16[512,1024]{1,0:T(8,128)(2,1)S(1)}, bf16[512,1024]{1,0:T(8,128)(2,1)}, u32[]{:S(2)}) copy-start(bf16[512,1024]{1,0:T(8,128)(2,1)} %param.12) | copy-start | bytes 3145732
  219.7 12.4 %copy-start.5 = (f32[1024]{0:T(1024)S(1)}, f32[1024]{0:T(1024)}, u32[]{:S(2)}) copy-start(f32[1024]{0:T(1024)} %param.19) | copy-start | bytes 12292
  219.7 25.9 %all-gather.17.cloned.1.call-start = ((), (), s32[]{:S(2)}) async-start(), calls=%async_computation.7 | async-start | bytes 3145728 | tf_op jit(solution)/shard_map/all_gather | solution.py:66
  227.6 4.4 copy-start.2
  233.6 157.4 %all-gather.19.cloned.1.call-start = ((), (), s32[]{:S(2)}) async-start(), calls=%async_computation.8 | async-start | bytes 12255232 | tf_op jit(solution)/shard_map/all_gather | solution.py:71
  234.3 299.1 %all-gather.21.cloned.1.call-start = ((), (), s32[]{:S(2)}) async-start(), calls=%async_computation.9 | async-start | bytes 12255232 | tf_op jit(solution)/shard_map/all_gather | solution.py:72
  235.1 481.3 %all-gather.23.cloned.1.call-start = ((), (), s32[]{:S(2)}) async-start(), calls=%async_computation.10 | async-start | bytes 12255232 | tf_op jit(solution)/shard_map/all_gather | solution.py:76
  235.8 511.3 %reduce-scatter.5.cloned.1.call-start = ((), (), s32[]{:S(2)}) async-start(), calls=%async_computation.11 | async-start | bytes 3145728 | tf_op jit(solution)/shard_map/reduce_scatter | solution.py:79
  245.6 470.8 %copy-start.9 = (bf16[512,2048]{1,0:T(8,128)(2,1)S(1)}, bf16[512,2048]{1,0:T(8,128)(2,1)}, u32[]{:S(2)}) copy-start(bf16[512,2048]{1,0:T(8,128)(2,1)} %all-gather.17.cloned.1.call-done) | copy-start | bytes 6291460
  739.1 8.0 %copy-start = (bf16[512,1024]{1,0:T(8,128)(2,1)S(1)}, bf16[512,1024]{1,0:T(8,128)(2,1)}, u32[]{:S(2)}) copy-start(bf16[512,1024]{1,0:T(8,128)(2,1)} %multiply_convert_fusion.2) | copy-start | bytes 3145732
  739.1 12.4 %copy-start.6 = (f32[1024]{0:T(1024)S(1)}, f32[1024]{0:T(1024)}, u32[]{:S(2)}) copy-start(f32[1024]{0:T(1024)} %param.23) | copy-start | bytes 12292
  747.1 4.4 copy-start.3
Sparse Core Ops, SparseCore 0:
  8.9 13.2 all-gather.8
  25.0 61.5 all-gather.12
  89.3 59.1 all-gather.10
  151.1 61.7 all-gather.14
  219.8 7.7 reduce-scatter.2
  233.7 11.8 all-gather.16
  248.3 142.5 all-gather.18
  393.7 139.6 all-gather.20
  536.1 180.2 all-gather.22
  739.3 7.7 reduce-scatter.4
where the time goes:
time: 760 us
  waiting for transfers between devices  684 us (90%)
  matrix products  46.3 us (6%)
  between operations  13.6 us (2%)
    all_gather x1, waiting for transfers between devices, on_device(): lax.all_gather(down_weight, 'fs', axis=1, tiled=True)  183 us
    all_gather x1, waiting for transfers between devices, on_device(): gate = add_first(lax.all_gather(gate_weight, 'fs', axis=0, tiled=True))  145 us
    all_gather x1, waiting for transfers between devices, on_device(): upper = add_first(lax.all_gather(up_weight, 'fs', axis=0, tiled=True))  130 us
    all_gather x1, waiting for transfers between devices, on_device(): pre_v = add_one(lax.all_gather(v_weight, 'fs', axis=0, tiled=True))  64.4 us
    all_gather x1, waiting for transfers between devices, on_device(): lax.all_gather(out_weight, 'fs', axis=1, tiled=True)  64.3 us
    all_gather x1, waiting for transfers between devices, on_device(): pre_u = add_one(lax.all_gather(u_weight, 'fs', axis=0, tiled=True))  54.1 us
    dot_general x1, matrix products, on_device(): jnp.dot(hidden, lax.all_gather(down_weight, 'fs', axis=1, tiled=True), pr...  22.8 us
    dot_general x2, matrix products, add_rows(): return jnp.dot(left, piece, preferred_element_type=jnp.float32)  16.3 us
  transfers between devices with their start and end apart: 10, of which 10 were waited for; matrix products, arithmetic and copies ran while one was open for 2% of the time, Pallas kernels for 0%

commit v1 on v0

--- a/solution.py
+++ b/solution.py
@@ -39,7 +39,11 @@
     def add_one(piece):
         return add_rows(whole, piece)
 
-    pre_u = add_one(lax.all_gather(u_weight, "fs", axis=0, tiled=True))
+    pre_u = add_one(
+        jnp.concatenate(
+            lax.all_to_all(jnp.stack([u_weight] * lax.axis_size("fs")), "fs", 0, 0), axis=0
+        )
+    )
     pre_v = add_one(lax.all_gather(v_weight, "fs", axis=0, tiled=True))
     gated = jax.nn.gelu(pre_u)
     valued = jax.nn.gelu(pre_v)

time: 760 us -> 709 us (0.933)
  waiting for transfers between devices: 684 us -> 618 us
  starting transfers between devices: 0.53 us -> 8.84 us
    all_gather x1 -> x0, waiting for transfers between devices: 54.1 us -> none  [on_device(): pre_u = add_one(lax.all_gather(u_weight, 'fs', axis=0, tiled=True))]
    all_gather x1, waiting for transfers between devices: 64.3 us -> 52 us  [on_device(): lax.all_gather(out_weight, 'fs', axis=1, tiled=True)]
    all_gather x1, waiting for transfers between devices: 64.4 us -> 75.7 us  [on_device(): pre_v = add_one(lax.all_gather(v_weight, 'fs', axis=0, tiled=True))]
    all_gather x1, waiting for transfers between devices: 12.8 us -> 2.58 us  [on_device(): whole = lax.all_gather(tokens, 'tp', axis=1, tiled=True)]
    all_to_all x0 -> x1, starting transfers between devices: none -> 8.34 us  [on_device(): lax.all_to_all(jnp.stack([u_weight] * lax.axis_size('fs')), 'fs', 0, 0)]
  transfers between devices with their start and end apart: 10 -> 10, of which waited for: 10 -> 9; matrix products, arithmetic and copies ran while one was open for 2% -> 4% of each run, Pallas kernels for 0% -> 0%
where the time goes in v1:
time: 709 us
  waiting for transfers between devices  618 us (87%)
  matrix products  47.7 us (7%)
  between operations  13.3 us (2%)
  starting transfers between devices  8.84 us (1%)
  other arithmetic  8.5 us (1%)
  blocking collectives  7.52 us (1%)
    all_gather x1, waiting for transfers between devices, on_device(): lax.all_gather(down_weight, 'fs', axis=1, tiled=True)  183 us
    all_gather x1, waiting for transfers between devices, on_device(): gate = add_first(lax.all_gather(gate_weight, 'fs', axis=0, tiled=True))  145 us
    all_gather x1, waiting for transfers between devices, on_device(): upper = add_first(lax.all_gather(up_weight, 'fs', axis=0, tiled=True))  130 us
    all_gather x1, waiting for transfers between devices, on_device(): pre_v = add_one(lax.all_gather(v_weight, 'fs', axis=0, tiled=True))  75.7 us
    all_gather x1, waiting for transfers between devices, on_device(): lax.all_gather(out_weight, 'fs', axis=1, tiled=True)  52 us
    dot_general x1, matrix products, on_device(): jnp.dot(hidden, lax.all_gather(down_weight, 'fs', axis=1, tiled=True), pr...  22.8 us
    dot_general x2, matrix products, add_rows(): return jnp.dot(left, piece, preferred_element_type=jnp.float32)  17.1 us
  transfers between devices with their start and end apart: 10, of which 9 were waited for; matrix products, arithmetic and copies ran while one was open for 4% of the time, Pallas kernels for 0%

profile of v1, /device:TPU:0, one launch (start us, length us, event | category | flops | bytes accessed | tf_op | source)
XLA Modules:
  0.0 708.5 jit_solution(5176097042439545202)
XLA Ops:
  6.5 0.0 all-gather.8.cloned.1.call-start
  6.5 0.7 all-gather.8.cloned.1.call-update
  7.3 0.0 all-gather.10.cloned.1.call-start
  7.3 0.7 all-gather.10.cloned.1.call-update
  8.0 2.4 stack.2
  10.5 8.3 %all-to-all-start = ((bf16[16,128,512]{2,1,0:T(8,128)(2,1)}), bf16[16,128,512]{2,1,0:T(8,128)(2,1)S(1)}, u32[]{:S(2)}, u32[]{:S(2)}) async-start(bf16[16,128,512]{2,1,0:T(8,128)(2,1)} %stack.2), calls=%async_computation | async-start | bytes 4194304 | tf_op jit(solution)/shard_map/all_to_all | solution.py:44
  18.8 0.0 all-gather.12.cloned.1.call-start
  18.8 0.7 all-gather.12.cloned.1.call-update
  19.5 0.0 reduce-scatter.3.cloned.1.call-start
  19.6 0.0 copy-start.7
  19.6 2.6 all-gather.8.cloned.1.call-done
  22.2 75.7 %all-gather.10.cloned.1.call-done = bf16[2048,512]{1,0:T(8,128)(2,1)} async-done(((bf16[128,512]{1,0:T(8,128)(2,1)}), bf16[2048,512]{1,0:T(8,128)(2,1)}) %all-gather.10.cloned.1.call-update) | async-done | bytes 2097168 | tf_op jit(solution)/shard_map/all_gather | solution.py:47
  97.9 4.6 fusion.35
  102.5 2.6 all-reduce.2
  105.1 1.7 multiply_convert_fusion.3
  106.7 0.9 reshape.47
  107.7 0.0 copy-done.4
  107.7 1.4 fusion.2
  109.1 1.3 copy.19
  110.4 0.0 all-to-all-done
  110.4 52.0 %all-gather.12.cloned.1.call-done = bf16[512,2048]{1,0:T(8,128)(2,1)} async-done(((bf16[512,128]{1,0:T(8,128)(2,1)}), bf16[512,2048]{1,0:T(8,128)(2,1)}) %all-gather.12.cloned.1.call-update) | async-done | bytes 2097168 | tf_op jit(solution)/shard_map/all_gather | solution.py:63
  162.3 6.5 convolution_convert_fusion.1
  168.8 0.0 reduce-scatter.3.cloned.1.call-update
  168.8 0.0 all-gather.14.cloned.1.call-start
  168.9 7.9 %reduce-scatter.3.cloned.1.call-done = bf16[512,1024]{1,0:T(8,128)(2,1)} async-done(((bf16[512,2048]{1,0:T(8,128)(2,1)}), bf16[512,1024]{1,0:T(8,128)(2,1)}) %reduce-scatter.3.cloned.1.call-update) | async-done | bytes 1048592 | tf_op jit(solution)/shard_map/reduce_scatter | solution.py:66
  176.8 1.9 fusion
  178.7 2.5 all-reduce.1
  181.2 0.0 copy-done.2
  181.2 1.5 multiply_convert_fusion.2
  182.7 0.0 all-gather.14.cloned.1.call-update
  182.7 0.0 all-gather.16.cloned.1.call-start
  182.8 0.5 all-gather.16.cloned.1.call-update
  183.3 0.0 all-gather.18.cloned.1.call-start
  183.3 0.7 all-gather.18.cloned.1.call-update
  184.0 0.0 all-gather.20.cloned.1.call-start
  184.1 0.7 all-gather.20.cloned.1.call-update
  184.8 0.2 reduce-scatter.5.cloned.1.call-start
  185.0 9.7 %all-gather.14.cloned.1.call-done = bf16[512,2048]{1,0:T(8,128)(2,1)} async-done(((bf16[512,1024]{1,0:T(8,128)(2,1)}), bf16[512,2048]{1,0:T(8,128)(2,1)}) %all-gather.14.cloned.1.call-update) | async-done | bytes 2097168 | tf_op jit(solution)/shard_map/all_gather | solution.py:70
  194.7 145.2 %all-gather.16.cloned.1.call-done = bf16[2048,2816]{1,0:T(8,128)(2,1)} async-done(((bf16[128,2816]{1,0:T(8,128)(2,1)}), bf16[2048,2816]{1,0:T(8,128)(2,1)}) %all-gather.16.cloned.1.call-update) | async-done | bytes 11534352 | tf_op jit(solution)/shard_map/all_gather | solution.py:75
  340.0 12.5 %fusion.38 = f32[512,2816]{1,0:T(8,128)} fusion(bf16[512,2048]{1,0:T(8,128)(2,1)} %all-gather.14.cloned.1.call-done, bf16[2048,2816]{1,0:T(8,128)(2,1)} %all-gather.16.cloned.1.call-done), kind=kOutput, calls=%fused_computation.57 | convolution fusion | flops 5905580032 | bytes 19398656 | tf_op jit(solution)/shard_map/dot_general | solution.py:11
  352.4 130.0 %all-gather.18.cloned.1.call-done = bf16[2048,2816]{1,0:T(8,128)(2,1)} async-done(((bf16[128,2816]{1,0:T(8,128)(2,1)}), bf16[2048,2816]{1,0:T(8,128)(2,1)}) %all-gather.18.cloned.1.call-update) | async-done | bytes 11534352 | tf_op jit(solution)/shard_map/all_gather | solution.py:76
  482.4 183.0 %all-gather.20.cloned.1.call-done = bf16[2816,2048]{1,0:T(8,128)(2,1)} async-done(((bf16[2816,128]{1,0:T(8,128)(2,1)}), bf16[2816,2048]{1,0:T(8,128)(2,1)}) %all-gather.20.cloned.1.call-update) | async-done | bytes 11534352 | tf_op jit(solution)/shard_map/all_gather | solution.py:80
  665.3 22.8 %convolution_convert_fusion = bf16[512,2048]{1,0:T(8,128)(2,1)} fusion(bf16[2816,2048]{1,0:T(8,128)(2,1)} %all-gather.20.cloned.1.call-done, f32[512,2816]{1,0:T(8,128)} %fusion.38, bf16[512,2048]{1,0:T(8,128)(2,1)S(1)} %copy-done.9, bf16[2048,2816]{1,0:T(8,128)(2,1)} %all-gather.18.cloned.1.call-done), kind=kOutput, calls=%fused_computation.1 | convolution fusion | flops 11820859392 | bytes 33030144 | tf_op jit(solution)/shard_map/dot_general | solution.py:78
  688.1 0.0 reduce-scatter.5.cloned.1.call-update
  688.1 8.0 %reduce-scatter.5.cloned.1.call-done = bf16[512,1024]{1,0:T(8,128)(2,1)} async-done(((bf16[512,2048]{1,0:T(8,128)(2,1)}), bf16[512,1024]{1,0:T(8,128)(2,1)}) %reduce-scatter.5.cloned.1.call-update) | async-done | bytes 1048592 | tf_op jit(solution)/shard_map/reduce_scatter | solution.py:83
  696.1 1.9 fusion.1
  698.0 2.5 all-reduce
  700.5 1.5 multiply_convert_fusion.1
  (21 shorter events, 0.1 us)
Async XLA Ops:
  6.5 15.7 %all-gather.8.cloned.1.call-start = ((), (), s32[]{:S(2)}) async-start(), calls=%async_computation.3 | async-start | bytes 3145728 | tf_op jit(solution)/shard_map/all_gather | solution.py:35
  7.3 90.6 %all-gather.10.cloned.1.call-start = ((), (), s32[]{:S(2)}) async-start(), calls=%async_computation.4 | async-start | bytes 2228224 | tf_op jit(solution)/shard_map/all_gather | solution.py:47
  10.5 99.9 %all-to-all-start = ((bf16[16,128,512]{2,1,0:T(8,128)(2,1)}), bf16[16,128,512]{2,1,0:T(8,128)(2,1)S(1)}, u32[]{:S(2)}, u32[]{:S(2)}) async-start(bf16[16,128,512]{2,1,0:T(8,128)(2,1)} %stack.2), calls=%async_computation | async-start | bytes 4194304 | tf_op jit(solution)/shard_map/all_to_all | solution.py:44
  18.8 143.5 %all-gather.12.cloned.1.call-start = ((), (), s32[]{:S(2)}) async-start(), calls=%async_computation.5 | async-start | bytes 2228224 | tf_op jit(solution)/shard_map/all_gather | solution.py:63
  19.5 157.3 %reduce-scatter.3.cloned.1.call-start = ((), (), s32[]{:S(2)}) async-start(), calls=%async_computation.6 | async-start | bytes 3145728 | tf_op jit(solution)/shard_map/reduce_scatter | solution.py:66
  19.6 85.5 %copy-start.7 = (f32[512]{0:T(512)S(1)}, f32[512]{0:T(512)}, u32[]{:S(2)}) copy-start(f32[512]{0:T(512)} %param.15) | copy-start | bytes 6148
  102.5 5.2 copy-start.4
  102.5 5.2 copy-start.8
  168.8 8.0 %copy-start.1 = (bf16[512,1024]{1,0:T(8,128)(2,1)S(1)}, bf16[512,1024]{1,0:T(8,128)(2,1)}, u32[]{:S(2)}) copy-start(bf16[512,1024]{1,0:T(8,128)(2,1)} %param.12) | copy-start | bytes 3145732
  168.8 12.4 %copy-start.5 = (f32[1024]{0:T(1024)S(1)}, f32[1024]{0:T(1024)}, u32[]{:S(2)}) copy-start(f32[1024]{0:T(1024)} %param.19) | copy-start | bytes 12292
  168.8 25.9 %all-gather.14.cloned.1.call-start = ((), (), s32[]{:S(2)}) async-start(), calls=%async_computation.7 | async-start | bytes 3145728 | tf_op jit(solution)/shard_map/all_gather | solution.py:70
  176.8 4.4 copy-start.2
  182.7 157.2 %all-gather.16.cloned.1.call-start = ((), (), s32[]{:S(2)}) async-start(), calls=%async_computation.8 | async-start | bytes 12255232 | tf_op jit(solution)/shard_map/all_gather | solution.py:75
  183.3 299.1 %all-gather.18.cloned.1.call-start = ((), (), s32[]{:S(2)}) async-start(), calls=%async_computation.9 | async-start | bytes 12255232 | tf_op jit(solution)/shard_map/all_gather | solution.py:76
  184.0 481.3 %all-gather.20.cloned.1.call-start = ((), (), s32[]{:S(2)}) async-start(), calls=%async_computation.10 | async-start | bytes 12255232 | tf_op jit(solution)/shard_map/all_gather | solution.py:80
  184.8 511.3 %reduce-scatter.5.cloned.1.call-start = ((), (), s32[]{:S(2)}) async-start(), calls=%async_computation.11 | async-start | bytes 3145728 | tf_op jit(solution)/shard_map/reduce_scatter | solution.py:83
  194.7 470.6 %copy-start.9 = (bf16[512,2048]{1,0:T(8,128)(2,1)S(1)}, bf16[512,2048]{1,0:T(8,128)(2,1)}, u32[]{:S(2)}) copy-start(bf16[512,2048]{1,0:T(8,128)(2,1)} %all-gather.14.cloned.1.call-done) | copy-start | bytes 6291460
  688.1 8.0 %copy-start = (bf16[512,1024]{1,0:T(8,128)(2,1)S(1)}, bf16[512,1024]{1,0:T(8,128)(2,1)}, u32[]{:S(2)}) copy-start(bf16[512,1024]{1,0:T(8,128)(2,1)} %multiply_convert_fusion.2) | copy-start | bytes 3145732
  688.1 12.4 %copy-start.6 = (f32[1024]{0:T(1024)S(1)}, f32[1024]{0:T(1024)}, u32[]{:S(2)}) copy-start(f32[1024]{0:T(1024)} %param.23) | copy-start | bytes 12292
  696.1 4.4 copy-start.3
Sparse Core Ops, SparseCore 0:
  8.9 13.2 all-gather.7
  25.0 72.8 all-gather.9
  100.6 61.7 all-gather.11
  169.0 7.7 reduce-scatter.2
  182.8 11.8 all-gather.13
  197.3 142.5 all-gather.15
  342.7 139.6 all-gather.17
  485.1 180.2 all-gather.19
  688.3 7.7 reduce-scatter.4
